TPU v7x, 32 devices: a whole 2x2x4 slice. The times are simulated.
32 devices in a mesh: grp: 2 (over y), sp: 4 (over z), tp: 4 (over x, core).
Axes of the slice: x: 2, y: 2, z: 4, core: 2. Of those that a mesh axis runs over, the one named last changes fastest.
Arguments:
- carryover_vector: bfloat16 [2048, 2048], P(('grp', 'sp', 'tp')), parts along dimension 0, may hold values from -6 to 6
- channel_source_entries: bfloat16 [2048, 1024], P(('grp', 'sp'), 'tp'), parts along dimension 0, may hold values from -6 to 6
- final_modulation_vector: bfloat16 [2048, 1024], P(('grp', 'sp'), 'tp'), parts along dimension 0, may hold values from -54 to 54
- entering_basis_matrix: bfloat16 [2048, 512], P(('grp', 'sp'), 'tp'), parts along dimension 0, may hold values from -6 to 6
- readout_basis_matrix: bfloat16 [2048, 512], P(('grp', 'sp'), 'tp'), parts along dimension 0, may hold values from -6 to 6
- raw_stride_amount: float32 [2048, 16], P(('grp', 'sp'), 'tp'), parts along dimension 0, may hold values from -6 to 5
- extra_log_attenuation: float32 [2048, 16], P(('grp', 'sp'), 'tp'), parts along dimension 0, may hold values from -1.4 to 0
- channel_fading_rate: float32 [16], P('tp'), may hold values from 0 to 0.1, as said below
- channel_source_kernel: float32 [4, 1024], P(None, 'tp'), may hold values from -3 to 3
- entering_basis_kernel: float32 [4, 512], P(None, 'tp'), may hold values from -3 to 3
- readout_basis_kernel: float32 [4, 512], P(None, 'tp'), may hold values from -3 to 3
- modulated_rescaling_vector: float32 [1024], replicated, may hold values from 0.1 to 1.9
- blender_final_matrix: bfloat16 [1024, 2048], replicated, may hold values from -0.1875 to 0.1875
- specialist_rescaling_vector: float32 [2048], replicated, may hold values from 0.1 to 1.9
- specialist_gating_matrices: bfloat16 [8, 2048, 1024], P('sp', None, 'tp'), may hold values from -0.125 to 0.125
- widening_matrices: bfloat16 [8, 2048, 1024], P('sp', None, 'tp'), may hold values from -0.125 to 0.125
- contracting_matrices: bfloat16 [8, 1024, 2048], P('sp', 'tp'), may hold values from -0.1875 to 0.1875
- assigned_specialist_ids: int32 [2048, 2], P(('grp', 'sp')), parts along dimension 0, may hold values from 0 to 7, as said below
- specialist_choice_affinity: float32 [2048, 2], P(('grp', 'sp', 'tp')), parts along dimension 0, may hold values from -6 to 6
- cluster_chance: float32 [2048], P(('grp', 'sp', 'tp')), parts along dimension 0, may hold values from 0.25 to 1
Outputs:
- layer_out: bfloat16 [2048, 2048], P(('grp', 'sp', 'tp')), parts along dimension 0
There are 2 independent parts, one for each index of `grp`. A program takes and returns all parts, laid end to end along the dimension named above; an argument that names none is the same for every part. Nothing has to cross between parts.
Inputs may be any that keep to these rules, and one draw needn't show every extreme that they name: `assigned_specialist_ids`: each row names 2 different experts of one group: the experts g * 2 to (g + 1) * 2 - 1 for one g below 4. In each aligned block of 64 rows (the rows of one device) no expert is named by more than 32 rows, and every expert of one group, the same group in all blocks, is named by exactly 32 rows of every block. `channel_fading_rate`: positive.
All inputs are finite; a program needn't handle non-finite values.
Results may differ from a plain program's by a relative error of at most 0.015.
Values may be sent and summed in bfloat16 or wider, within the bound.
A program may use at most 64 MiB of HBM per device.

v0:
```python
import jax
import jax.numpy as jnp
from jax import lax
from jax.sharding import PartitionSpec as P

HEAD_DIM = 64
STATE = 128
BLOCK = 64


EPS = 1e-06
HIGHEST = lax.Precision.HIGHEST


def prefix(x, axis, combine, identity):
    size, index = (lax.axis_size(axis), lax.axis_index(axis))
    everything = jax.tree.map(
        lambda part, kind: lax.all_gather(part.astype(kind), axis), x, (jnp.bfloat16, jnp.bfloat16)
    )
    start = jax.tree.map(
        lambda part, zero: jnp.broadcast_to(jnp.asarray(zero, part.dtype), part.shape), x, identity
    )

    def lap(k, before):
        reached = k < index
        new = combine(
            before, jax.tree.map(lambda part, own: part[k].astype(own.dtype), everything, x)
        )
        return jax.tree.map(lambda a, b: jnp.where(reached, a, b), new, before)

    return lax.fori_loop(0, size, lap, start)


def from_behind(x, axis, by):
    size = lax.axis_size(axis)
    pairs = [(i, i + by) for i in range(size) if 0 <= i + by < size]
    return lax.ppermute(x, axis, pairs)


def causal_conv(signal, earlier, weights):
    kernel_len = weights.shape[0]
    length = signal.shape[0]
    joined = jnp.concatenate([earlier, signal], axis=0).astype(jnp.float32)
    accumulated = jnp.zeros((length, signal.shape[1]), jnp.float32)
    for offset in range(kernel_len):
        accumulated = accumulated + weights[offset][None, :] * joined[offset : offset + length]
    return jax.nn.silu(accumulated)


def link_states(earlier, later):
    return (earlier[0] * later[0], earlier[1] * later[0][..., None, None] + later[1])


def device_states(scaled_in, log_attenuation, keys_b, queries_c, groups_here):
    length = scaled_in.shape[0]
    blocks = length // BLOCK
    per_group = scaled_in.shape[1] // groups_here
    scaled_in = scaled_in.reshape(blocks, BLOCK, groups_here, per_group, HEAD_DIM)
    log_attenuation = log_attenuation.reshape(blocks, BLOCK, groups_here, per_group)
    keys_b = keys_b.reshape(blocks, BLOCK, groups_here, STATE)
    queries_c = queries_c.reshape(blocks, BLOCK, groups_here, STATE)
    running = jnp.cumsum(log_attenuation, axis=1)
    lower_mask = jnp.tril(jnp.ones((BLOCK, BLOCK), dtype=bool))
    between = running[:, :, None] - running[:, None, :]
    decays = jnp.exp(jnp.where(lower_mask[None, :, :, None, None], between, -jnp.inf))
    scores = jnp.einsum("blgn,bsgn->blsg", queries_c, keys_b, precision=HIGHEST)
    inside = jnp.einsum("blsg,blsgr,bsgrp->blgrp", scores, decays, scaled_in, precision=HIGHEST)
    totals = running[:, -1]
    remain = jnp.exp(totals[:, None] - running)
    block_states = jnp.einsum(
        "bsgn,bsgr,bsgrp->bgrpn", keys_b, remain, scaled_in, precision=HIGHEST
    )

    def advance(carried, pieces):
        return (carried * jnp.exp(pieces[1])[..., None, None] + pieces[0], carried)

    initial = jnp.zeros(block_states.shape[1:], jnp.float32)
    own_state, entering = lax.scan(advance, initial, (block_states, totals))
    own_decay = jnp.exp(jnp.sum(totals, axis=0))
    _, incoming = prefix(
        (own_decay, own_state),
        "sp",
        link_states,
        (jnp.ones_like(own_decay), jnp.zeros_like(own_state)),
    )
    preceding = jnp.exp(jnp.cumsum(totals, axis=0) - totals)
    entering = entering + preceding[..., None, None] * incoming[None]
    outside = jnp.einsum(
        "blgn,bgrpn,blgr->blgrp", queries_c, entering, jnp.exp(running), precision=HIGHEST
    )
    return (inside + outside).reshape(length, -1)


def fetch_rows(tokens, sources):
    present = sources >= 0
    picked = jnp.take(tokens, jnp.maximum(sources, 0), axis=0)
    return jnp.where(present[:, None], picked, jnp.zeros_like(picked))


def slot_tables(chosen_ids, quarters, row_count, experts, capacity):
    picks = chosen_ids.shape[1]
    flat_ids = chosen_ids.reshape(quarters, row_count * picks)
    member = (flat_ids[..., None] == jnp.arange(experts, dtype=jnp.int32)).astype(jnp.int32)
    position = jnp.sum((jnp.cumsum(member, axis=1) - member) * member, axis=2)
    quarter_ids = jnp.arange(quarters, dtype=jnp.int32)[:, None]
    slot_index = flat_ids * (quarters * capacity) + quarter_ids * capacity + position
    token_index = (
        quarter_ids * row_count + jnp.arange(row_count * picks, dtype=jnp.int32)[None, :] // picks
    )
    sources = (
        jnp.full((experts * quarters * capacity,), -1, jnp.int32)
        .at[slot_index.reshape(-1)]
        .set(token_index.reshape(-1))
    )
    return (sources, position)


def per_device(
    carryover_vector,
    channel_source_entries,
    final_modulation_vector,
    entering_basis_matrix,
    readout_basis_matrix,
    raw_stride_amount,
    extra_log_attenuation,
    channel_fading_rate,
    channel_source_kernel,
    entering_basis_kernel,
    readout_basis_kernel,
    modulated_rescaling_vector,
    blender_final_matrix,
    specialist_rescaling_vector,
    specialist_gating_matrices,
    widening_matrices,
    contracting_matrices,
    assigned_specialist_ids,
    specialist_choice_affinity,
    cluster_chance,
):
    length = channel_source_entries.shape[0]
    row_count = carryover_vector.shape[0]
    model_width = carryover_vector.shape[1]
    heads_here = channel_fading_rate.shape[0]
    groups_here = entering_basis_matrix.shape[1] // STATE
    tp_index = lax.axis_index("tp")
    rim_rows = channel_source_kernel.shape[0] - 1
    neighbours = from_behind(
        (
            channel_source_entries[length - rim_rows :],
            entering_basis_matrix[length - rim_rows :],
            readout_basis_matrix[length - rim_rows :],
        ),
        "sp",
        1,
    )
    inputs_x = causal_conv(channel_source_entries, neighbours[0], channel_source_kernel)
    keys_b = causal_conv(entering_basis_matrix, neighbours[1], entering_basis_kernel)
    queries_c = causal_conv(readout_basis_matrix, neighbours[2], readout_basis_kernel)
    channel_stride_amount = jax.nn.softplus(raw_stride_amount)
    log_attenuation = extra_log_attenuation - channel_fading_rate[None, :] * channel_stride_amount
    heads_x = inputs_x.reshape(length, heads_here, HEAD_DIM)
    mixed = device_states(
        heads_x * channel_stride_amount[:, :, None], log_attenuation, keys_b, queries_c, groups_here
    )
    gated = mixed * jax.nn.silu(final_modulation_vector.astype(jnp.float32))
    head_cols = gated.shape[1]
    squares = lax.psum(jnp.sum(gated * gated, axis=1), "tp")
    first_col = tp_index * head_cols
    gain_part = lax.dynamic_slice_in_dim(modulated_rescaling_vector, first_col, head_cols, 0)
    scale = lax.rsqrt(squares / (head_cols * lax.axis_size("tp")) + EPS)
    normed = (gated * scale[:, None] * gain_part[None, :]).astype(jnp.bfloat16)
    weight_rows = lax.dynamic_slice_in_dim(blender_final_matrix, first_col, head_cols, 0)
    summed = lax.psum_scatter(
        jnp.dot(normed, weight_rows, preferred_element_type=jnp.float32).astype(jnp.bfloat16),
        "tp",
        scatter_dimension=0,
        tiled=True,
    ).astype(jnp.float32)
    middle = (carryover_vector.astype(jnp.float32) + summed).astype(jnp.bfloat16)
    middle_wide = middle.astype(jnp.float32)
    expert_input = (
        middle_wide
        * lax.rsqrt(jnp.mean(middle_wide * middle_wide, axis=1, keepdims=True) + EPS)
        * specialist_rescaling_vector[None, :]
    ).astype(jnp.bfloat16)
    sp_count = lax.axis_size("sp")
    local_experts = specialist_gating_matrices.shape[0]
    experts = sp_count * local_experts
    picks = assigned_specialist_ids.shape[1]
    capacity = 2 * row_count * picks // experts
    own_ids = lax.dynamic_slice_in_dim(assigned_specialist_ids, tp_index * row_count, row_count, 0)
    sources, position = slot_tables(own_ids, 1, row_count, experts, capacity)
    own_position = position[0]
    outgoing = fetch_rows(expert_input, sources).reshape(
        sp_count, local_experts, 1, capacity, model_width
    )
    received = lax.all_to_all(outgoing, "sp", split_axis=0, concat_axis=0, tiled=True)
    arrived = lax.all_gather(received, "tp", axis=2, tiled=True)
    gate_value = jnp.einsum(
        "slqcd,ldf->slqcf", arrived, specialist_gating_matrices, preferred_element_type=jnp.float32
    )
    up_value = jnp.einsum(
        "slqcd,ldf->slqcf", arrived, widening_matrices, preferred_element_type=jnp.float32
    )
    hidden = (jax.nn.silu(gate_value) * up_value).astype(jnp.bfloat16)
    partial_value = jnp.einsum(
        "slqcf,lfd->slqcd", hidden, contracting_matrices, preferred_element_type=jnp.float32
    )
    width_total = lax.psum_scatter(
        partial_value.astype(jnp.bfloat16), "tp", scatter_dimension=2, tiled=True
    )
    returned = lax.all_to_all(width_total, "sp", split_axis=0, concat_axis=0, tiled=True)
    answers = returned.reshape(experts * capacity, model_width)
    own_slots = own_ids.reshape(-1) * capacity + own_position
    gathered = (
        jnp.take(answers, own_slots, axis=0)
        .reshape(row_count, picks, model_width)
        .astype(jnp.float32)
    )
    lifted = jnp.exp(specialist_choice_affinity)
    shares = cluster_chance[:, None] * lifted / jnp.sum(lifted, axis=1, keepdims=True)
    return (middle_wide + jnp.sum(shares[:, :, None] * gathered, axis=1)).astype(jnp.bfloat16)


def solution(mesh):
    return jax.shard_map(
        per_device,
        mesh=mesh,
        in_specs=(
            P(("grp", "sp", "tp"), None),
            P(("grp", "sp"), "tp"),
            P(("grp", "sp"), "tp"),
            P(("grp", "sp"), "tp"),
            P(("grp", "sp"), "tp"),
            P(("grp", "sp"), "tp"),
            P(("grp", "sp"), "tp"),
            P("tp"),
            P(None, "tp"),
            P(None, "tp"),
            P(None, "tp"),
            P(),
            P(),
            P(),
            P("sp", None, "tp"),
            P("sp", None, "tp"),
            P("sp", "tp", None),
            P(("grp", "sp"), None),
            P(("grp", "sp", "tp"), None),
            P(("grp", "sp", "tp")),
        ),
        out_specs=P(("grp", "sp", "tp"), None),
        check_vma=False,
    )
```

profile of v0, /device:TPU:0, one launch (start us, length us, event | category | flops | bytes accessed | tf_op | source)
XLA Modules:
  0.0 319.8 jit_solution(16256433366509483427)
XLA Ops:
  6.5 0.8 slice.103
  7.4 4.9 %collective-permute-start.2 = (bf16[3,256]{1,0:T(4,128)(2,1)S(1)}, bf16[3,256]{1,0:T(4,128)(2,1)S(1)}, u32[]{:S(2)}, u32[]{:S(2)}) collective-permute-start(bf16[3,256]{1,0:T(4,128)(2,1)S(1)} %slice.103), channel_id=1, source_target_pairs={{0,4},{4,8},{8,12},{1,5},{5,9},{9,13},{2,6},{6,10},{10,14},{3,7},{... | collective-permute-start | bytes 4616 | tf_op jit(solution)/shard_map/ppermute | solution.py:37
  12.3 0.7 slice.85
  13.0 3.5 %collective-permute-start = (bf16[3,128]{1,0:T(4,128)(2,1)S(1)}, bf16[3,128]{1,0:T(4,128)(2,1)S(1)}, u32[]{:S(2)}, u32[]{:S(2)}) collective-permute-start(bf16[3,128]{1,0:T(4,128)(2,1)S(1)} %slice.85), channel_id=1, source_target_pairs={{0,4},{4,8},{8,12},{1,5},{5,9},{9,13},{2,6},{6,10},{10,14},{3,7},{... | collective-permute-start | bytes 2312 | tf_op jit(solution)/shard_map/ppermute | solution.py:37
  16.5 0.7 slice.94
  17.2 3.5 %collective-permute-start.1 = (bf16[3,128]{1,0:T(4,128)(2,1)S(1)}, bf16[3,128]{1,0:T(4,128)(2,1)S(1)}, u32[]{:S(2)}, u32[]{:S(2)}) collective-permute-start(bf16[3,128]{1,0:T(4,128)(2,1)S(1)} %slice.94), channel_id=1, source_target_pairs={{0,4},{4,8},{8,12},{1,5},{5,9},{9,13},{2,6},{6,10},{10,14},{3,7},{... | collective-permute-start | bytes 2312 | tf_op jit(solution)/shard_map/ppermute | solution.py:37
  20.7 0.6 iota_compare_fusion.1
  21.3 0.8 fusion.74
  22.1 0.8 slice_bitcast_fusion.7
  23.0 0.8 compare_select_fusion
  24.0 0.6 slice_reduce_fusion
  24.7 0.7 copy.81
  25.5 1.2 dynamic-slice
  27.7 8.4 %all-reduce = bf16[16]{0:T(256)(128)(2,1)S(1)} all-reduce(bf16[16]{0:T(256)(128)(2,1)S(1)} %dynamic-update-slice), channel_id=2, replica_groups=mesh['grp'=2,'sp'=4,'tp'=4] {'sp'}, use_global_device_ids=true, to_apply=%add | all-reduce | flops 16 | bytes 64
  36.0 0.7 reshape.446
  36.7 0.8 slice_bitcast_fusion.3
  37.6 0.6 subtract_exponential_fusion.1
  38.1 0.7 copy.80
  38.8 1.3 dynamic_slice.31
  40.2 0.9 maximum_convert_fusion.1
  41.2 0.9 maximum_convert_fusion.2
  42.5 0.8 copy.73
  43.3 0.9 maximum_convert_fusion
  44.8 1.5 convolution_bitcast_fusion
  46.4 5.6 %while.27 = (s32[]{:T(128)}, f32[1,4,64,128]{3,2,1,0:T(8,128)S(1)}, f32[4,1,4,64,128]{4,3,2,1,0:T(8,128)}, f32[4,1,4]{2,1,0:T(1,128)}, f32[4,1,4,64,128]{4,3,2,1,0:T(8,128)S(1)}, /*index=5*/s32[]{:T(128)}, s32[]{:T(128)}) while((s32[]{:T(128)}, f32[1,4,64,128]{3,2,1,0:T(8,128)S(1)}, f32[4,1,4,64,128]{4,3,2,1,0:T(8,128)}, ...), condition=%wide.region_2.3_spmd.clone, body=%wide.region_1.2_spmd.clone.sunk | while | flops 131075 | bytes 656016 | solution.py:78
  46.4 0.7 bitcast_dynamic-update-slice_fusion.2
  47.1 0.6 fusion.85
  47.8 0.7 bitcast_dynamic-update-slice_fusion.2
  48.4 0.7 fusion.85
  49.2 0.7 bitcast_dynamic-update-slice_fusion.2
  49.9 0.6 fusion.85
  50.6 0.7 bitcast_dynamic-update-slice_fusion.2
  51.3 0.6 fusion.85
  52.0 13.9 %all-gather.1 = bf16[4,4,64,128]{3,2,1,0:T(8,128)(2,1)S(1)} all-gather(bf16[1,4,64,128]{3,2,1,0:T(8,128)(2,1)S(1)} %convert_element_type.121), channel_id=3, replica_groups=mesh['grp'=2,'sp'=4,'tp'=4] {'sp'}, dimensions={0}, use_global_device_ids=true | all-gather | bytes 327680 | tf_op jit(solution)/shard_map/all_gather | solution.py:18
  66.0 3.0 while.28
  66.0 0.6 bitcast_convert_fusion.2
  66.7 0.6 bitcast_convert_fusion.2
  67.5 0.6 bitcast_convert_fusion.2
  68.2 0.7 bitcast_convert_fusion.2
  68.9 2.8 fusion.20
  71.7 2.0 fusion.21
  74.6 5.7 %psum.7 = f32[256]{0:T(256)S(1)} all-reduce(f32[256]{0:T(256)S(1)} %multiply_reduce_fusion.1), channel_id=1, replica_groups=mesh['grp'=2,'sp'=4,'tp'=4] {'tp'}, use_global_device_ids=true, to_apply=%region_8.9 | all-reduce | flops 256 | bytes 2048 | tf_op jit(solution)/shard_map/psum | solution.py:167
  80.3 2.7 convolution_convert_fusion
  84.1 1.0 scatter_custom_fusion
  85.3 22.6 %reduce-scatter.5.cloned.1.call-done = bf16[64,2048]{1,0:T(8,128)(2,1)} async-done(((bf16[256,2048]{1,0:T(8,128)(2,1)}), bf16[64,2048]{1,0:T(8,128)(2,1)}) %reduce-scatter.5.cloned.1.call-update) | async-done | bytes 262160 | tf_op jit(solution)/shard_map/reduce_scatter | solution.py:173
  108.0 1.1 fusion.25
  109.1 1.1 fusion.27
  110.2 1.4 gather_fusion
  111.8 30.0 %all_to_all.10 = bf16[4,2,1,32,2048]{4,3,2,1,0:T(8,128)(2,1)S(1)} all-to-all(bf16[4,2,1,32,2048]{4,3,2,1,0:T(8,128)(2,1)S(1)} %select_bitcast_fusion), channel_id=1, replica_groups=mesh['grp'=2,'sp'=4,'tp'=4] {'sp'}, dimensions={0} | all-to-all | bytes 2097152 | tf_op jit(solution)/shard_map/all_to_all | solution.py:197
  141.8 1.0 copy.93
  143.1 32.5 %all-gather.4.cloned.1.call-done = bf16[4,2,4,32,2048]{4,3,2,0,1:T(8,128)(2,1)} async-done(((bf16[4,2,1,32,2048]{4,3,2,0,1:T(8,128)(2,1)}), bf16[4,2,4,32,2048]{4,3,2,0,1:T(8,128)(2,1)}) %all-gather.4.cloned.1.call-update) | async-done | bytes 4194320 | tf_op jit(solution)/shard_map/all_gather | solution.py:198
  175.6 4.1 %fusion.8 = f32[4,2,4,32,256]{4,3,2,0,1:T(8,128)S(1)} fusion(bf16[4,2,4,32,2048]{4,3,2,0,1:T(8,128)(2,1)} %all-gather.4.cloned.1.call-done, bf16[2,2048,256]{2,1,0:T(8,128)(2,1)} %param.38), kind=kOutput, calls=%fused_computation.18 | convolution fusion | flops 1073741824 | bytes 7340032 | tf_op jit(solution)/shard_map/slqcd,ldf->slqcf/dot_general | solution.py:199
  179.7 7.3 %convert_bitcast_fusion = bf16[4,2,4,32,2048]{4,3,2,0,1:T(8,128)(2,1)} fusion(bf16[2,256,2048]{2,1,0:T(8,128)(2,1)S(1)} %copy-done, bf16[4,2,4,32,2048]{4,3,2,0,1:T(8,128)(2,1)} %all-gather.4.cloned.1.call-done, bf16[2,2048,256]{2,1,0:T(8,128)(2,1)} %param.39, f32[4,2,4,32,256]{4,3,2,0,1:T(8,128)S(1)} %fusion.8), kind=kOutput, calls=%fused_computation.11 | convolution fusion | flops 2151153664 | bytes 13631488 | tf_op jit(solution)/shard_map/slqcf,lfd->slqcd/dot_general | solution.py:206
  187.1 0.6 copy-done.10
  187.7 0.6 dynamic-slice.1
  188.3 84.4 %all-reduce.4.cloned.1.call-done = bf16[4,2,4,32,2048]{4,3,2,0,1:T(8,128)(2,1)} async-done(((bf16[4,2,4,32,2048]{4,3,2,0,1:T(8,128)(2,1)}), bf16[4,2,4,32,2048]{4,3,2,0,1:T(8,128)(2,1)}) %all-reduce.4.cloned.1.call-update) | async-done | bytes 4194320
  272.7 1.9 constant_dynamic-slice_fusion.1
  274.6 1.1 copy.94
  275.7 4.7 %all-to-all-start.1 = ((bf16[4,2,1,32,2048]{4,3,2,1,0:T(8,128)(2,1)}), bf16[4,2,1,32,2048]{4,3,2,1,0:T(8,128)(2,1)S(1)}, u32[]{:S(2)}, u32[]{:S(2)}) async-start(bf16[4,2,1,32,2048]{4,3,2,1,0:T(8,128)(2,1)} %copy.94), calls=%async_computation.2 | async-start | bytes 2097152 | tf_op jit(solution)/shard_map/all_to_all | solution.py:212
  280.9 24.9 %all-to-all-done.1 = bf16[4,2,1,32,2048]{4,3,2,1,0:T(8,128)(2,1)S(1)} async-done(((bf16[4,2,1,32,2048]{4,3,2,1,0:T(8,128)(2,1)}), bf16[4,2,1,32,2048]{4,3,2,1,0:T(8,128)(2,1)S(1)}, u32[]{:S(2)}, u32[]{:S(2)}) %all-to-all-start.1) | async-done | bytes 1048608 | tf_op jit(solution)/shard_map/all_to_all | solution.py:212
  305.8 1.7 gather_fusion.1
  307.5 1.4 gather.15
  308.9 2.5 multiply_reduce_fusion
  311.5 1.8 fusion.28
  (87 shorter events, 5.7 us)
Async XLA Ops:
  6.5 173.2 %copy-start = (bf16[2,256,2048]{2,1,0:T(8,128)(2,1)S(1)}, bf16[2,256,2048]{2,1,0:T(8,128)(2,1)}, u32[]{:S(2)}) copy-start(bf16[2,256,2048]{2,1,0:T(8,128)(2,1)} %param.40) | copy-start | bytes 6291460
  6.5 101.4 %reduce-scatter.5.cloned.1.call-start = ((), (), s32[]{:S(2)}) async-start(), calls=%async_computation.3 | async-start | bytes 1310720 | tf_op jit(solution)/shard_map/reduce_scatter | solution.py:173
  7.4 35.9 %collective-permute-start.2 = (bf16[3,256]{1,0:T(4,128)(2,1)S(1)}, bf16[3,256]{1,0:T(4,128)(2,1)S(1)}, u32[]{:S(2)}, u32[]{:S(2)}) collective-permute-start(bf16[3,256]{1,0:T(4,128)(2,1)S(1)} %slice.103), channel_id=1, source_target_pairs={{0,4},{4,8},{8,12},{1,5},{5,9},{9,13},{2,6},{6,10},{10,14},{3,7},{... | collective-permute-start | bytes 4616 | tf_op jit(solution)/shard_map/ppermute | solution.py:37
  13.0 27.1 %collective-permute-start = (bf16[3,128]{1,0:T(4,128)(2,1)S(1)}, bf16[3,128]{1,0:T(4,128)(2,1)S(1)}, u32[]{:S(2)}, u32[]{:S(2)}) collective-permute-start(bf16[3,128]{1,0:T(4,128)(2,1)S(1)} %slice.85), channel_id=1, source_target_pairs={{0,4},{4,8},{8,12},{1,5},{5,9},{9,13},{2,6},{6,10},{10,14},{3,7},{... | collective-permute-start | bytes 2312 | tf_op jit(solution)/shard_map/ppermute | solution.py:37
  17.2 24.0 %collective-permute-start.1 = (bf16[3,128]{1,0:T(4,128)(2,1)S(1)}, bf16[3,128]{1,0:T(4,128)(2,1)S(1)}, u32[]{:S(2)}, u32[]{:S(2)}) collective-permute-start(bf16[3,128]{1,0:T(4,128)(2,1)S(1)} %slice.94), channel_id=1, source_target_pairs={{0,4},{4,8},{8,12},{1,5},{5,9},{9,13},{2,6},{6,10},{10,14},{3,7},{... | collective-permute-start | bytes 2312 | tf_op jit(solution)/shard_map/ppermute | solution.py:37
  41.1 1.0 copy-start.3
  52.0 22.5 %copy-start.4 = (bf16[256,256]{1,0:T(8,128)(2,1)S(1)}, bf16[256,256]{1,0:T(8,128)(2,1)}, u32[]{:S(2)}) copy-start(bf16[256,256]{1,0:T(8,128)(2,1)} %param.26) | copy-start | bytes 393220
  52.0 28.3 %copy-start.7 = (f32[256]{0:T(256)S(1)}, f32[256]{0:T(256)}, u32[]{:S(2)}) copy-start(f32[256]{0:T(256)} %dynamic_slice.31) | copy-start | bytes 3076
  68.9 14.2 %copy-start.8 = (s32[256,2]{0,1:T(2,128)S(1)}, s32[256,2]{0,1:T(2,128)}, u32[]{:S(2)}) copy-start(s32[256,2]{0,1:T(2,128)} %param.41) | copy-start | bytes 6148
  71.7 36.3 %copy-start.1 = (bf16[64,2048]{1,0:T(8,128)(2,1)S(1)}, bf16[64,2048]{1,0:T(8,128)(2,1)}, u32[]{:S(2)}) copy-start(bf16[64,2048]{1,0:T(8,128)(2,1)} %param.24) | copy-start | bytes 786436
  71.7 37.4 %copy-start.5 = (f32[2048]{0:T(1024)S(1)}, f32[2048]{0:T(1024)}, u32[]{:S(2)}) copy-start(f32[2048]{0:T(1024)} %param.37) | copy-start | bytes 24580
  83.1 92.5 %all-gather.4.cloned.1.call-start = ((), (), s32[]{:S(2)}) async-start(), calls=%async_computation.4 | async-start | bytes 5242880 | tf_op jit(solution)/shard_map/all_gather | solution.py:198
  142.8 129.8 %all-reduce.4.cloned.1.call-start = ((), (), s32[]{:S(2)}) async-start(), calls=%async_computation.5 | async-start | bytes 8388608
  187.0 0.7 copy-start.10
  187.0 93.7 %copy-start.6 = (f32[64,2]{0,1:T(2,128)S(1)}, f32[64,2]{0,1:T(2,128)}, u32[]{:S(2)}) copy-start(f32[64,2]{0,1:T(2,128)} %param.42) | copy-start | bytes 1540
  187.1 93.7 %copy-start.9 = (f32[64]{0:T(128)S(1)}, f32[64]{0:T(128)}, u32[]{:S(2)}) copy-start(f32[64]{0:T(128)} %param.43) | copy-start | bytes 772
  275.7 35.8 %copy-start.2 = (bf16[64,2048]{1,0:T(8,128)(2,1)S(1)}, bf16[64,2048]{1,0:T(8,128)(2,1)}, u32[]{:S(2)}) copy-start(bf16[64,2048]{1,0:T(8,128)(2,1)} %param.24) | copy-start | bytes 786436
  275.7 30.1 %all-to-all-start.1 = ((bf16[4,2,1,32,2048]{4,3,2,1,0:T(8,128)(2,1)}), bf16[4,2,1,32,2048]{4,3,2,1,0:T(8,128)(2,1)S(1)}, u32[]{:S(2)}, u32[]{:S(2)}) async-start(bf16[4,2,1,32,2048]{4,3,2,1,0:T(8,128)(2,1)} %copy.94), calls=%async_computation.2 | async-start | bytes 2097152 | tf_op jit(solution)/shard_map/all_to_all | solution.py:212
Sparse Core Ops, SparseCore 0:
  83.2 24.7 reduce-scatter.4
  143.0 32.5 all-gather.3
  187.2 85.4 all-reduce.3
where the time goes:
time: 321 us; the launch traced here: 320 us
  waiting for transfers between devices  165 us (51%)
  blocking collectives  57.9 us (18%)
  local copies, waits for them, and re-layouts  26.1 us (8%)
  matrix products  20.8 us (6%)
  other arithmetic  19.1 us (6%)
  starting transfers between devices  16.9 us (5%)
  between operations  14.2 us (4%)
    unnamed x4, waiting for transfers between devices  84.5 us
    all_gather x1, waiting for transfers between devices, per_device(): arrived = lax.all_gather(received, 'tp', axis=2, tiled=True)  32.5 us
    all_to_all x1, blocking collectives, per_device(): lax.all_to_all(outgoing, 'sp', split_axis=0, concat_axis=0, tiled=True)  30 us
    all_to_all x1, waiting for transfers between devices, per_device(): lax.all_to_all(width_total, 'sp', split_axis=0, concat_axis=0, tiled=True)  24.9 us
    reduce_scatter x1, waiting for transfers between devices, per_device(): lax.psum_scatter(jnp.dot(normed, weight_rows, preferred_element_type=jnp....  22.6 us
    all_gather x1, blocking collectives, prefix(): lax.all_gather(part.astype(kind), axis)  13.9 us
    ppermute x3, starting transfers between devices, from_behind(): return lax.ppermute(x, axis, pairs)  11.9 us
    unnamed x1, blocking collectives  8.36 us
  transfers between devices with their start and end apart: 7, of which 4 were waited for; matrix products, arithmetic and copies ran while one was open for 6% of the time, Pallas kernels for 0%

commit v1 on v0

v1 whole, which is shorter than its diff:
```python
import functools

import jax
import jax.numpy as jnp
from jax import lax
from jax.experimental import pallas as pl
from jax.experimental.pallas import tpu as pltpu
from jax.sharding import PartitionSpec as P

HEAD_DIM = 64
STATE = 128
EXPERT_GROUPS = 4
EPS = 1e-06
HIGHEST = lax.Precision.HIGHEST
F32 = jnp.float32
BF16 = jnp.bfloat16
TAIL = 16


def silu(v):
    return v / (1.0 + jnp.exp(-v))


def first_dims(a, b, precision=None):
    return lax.dot_general(
        a, b, (((0,), (0,)), ((), ())), precision=precision, preferred_element_type=F32
    )


def spread(cols, width):
    heads = cols.shape[1]
    lane_head = lax.broadcasted_iota(jnp.int32, (cols.shape[0], width), 1) // HEAD_DIM
    out = jnp.broadcast_to(cols[:, 0:1], (cols.shape[0], width))
    for h in range(1, heads):
        out = jnp.where(lane_head == h, cols[:, h : h + 1], out)
    return out


def routing(meta, first_expert, rows, cap, locals_):
    id0, id1 = meta[0:1, :rows], meta[1:2, :rows]
    hit0 = (id0 >= first_expert) & (id0 < first_expert + locals_)
    hit1 = (id1 >= first_expert) & (id1 < first_expert + locals_)
    hit = jnp.where(hit0 | hit1, 1.0, 0.0)
    earlier = lax.broadcasted_iota(jnp.int32, (rows, rows), 0) < lax.broadcasted_iota(
        jnp.int32, (rows, rows), 1
    )
    place = jnp.dot(
        jnp.broadcast_to(hit, (8, rows)).astype(BF16),
        jnp.where(earlier, 1.0, 0.0).astype(BF16),
        preferred_element_type=F32,
    )[0:1]
    slot = lax.broadcasted_iota(jnp.int32, (cap, rows), 0).astype(F32)
    return jnp.where((place == slot) & (hit > 0.5), 1.0, 0.0)


def kernel(
    n,
    tp,
    cap,
    x_ref,
    b_ref,
    c_ref,
    z_ref,
    raw_ref,
    extra_ref,
    fade_ref,
    kx_ref,
    kb_ref,
    kc_ref,
    gain_ref,
    blend_hbm,
    sgain_ref,
    wg_hbm,
    wu_hbm,
    wd_hbm,
    meta_ref,
    carry_ref,
    out_ref,
    blend,
    wg,
    wu,
    wd,
    tail_x,
    tail_b,
    tail_c,
    ext,
    st_send,
    tot_send,
    st_buf,
    tot_buf,
    g_send,
    g_buf,
    mid,
    metas,
    x_send,
    arr,
    part,
    rs1,
    far_send,
    rs2,
    ret_send,
    ret,
    local_sem,
    tail_ss,
    tail_rs,
    st_ss,
    st_rs,
    tot_ss,
    tot_rs,
    meta_ss,
    meta_rs,
    g_ss,
    g_rs,
    z_ss,
    z_rs,
    far_ss,
    far_rs,
    near_ss,
    near_rs,
    p1_ss,
    p1_rs,
    p2_ss,
    p2_rs,
    ret_ss,
    ret_rs,
):
    s = lax.axis_index("sp")
    t = lax.axis_index("tp")
    length, width = x_ref.shape
    rows, model = carry_ref.shape
    heads = width // HEAD_DIM
    locals_ = wg_hbm.shape[0]
    far = (t + tp // 2) % tp
    near = t + 1 - 2 * (t % 2)
    near_far = (near + tp // 2) % tp

    def remote(src, dst, ssem, rsem, sp, tpi):
        return pltpu.make_async_remote_copy(
            src_ref=src,
            dst_ref=dst,
            send_sem=ssem,
            recv_sem=rsem,
            device_id={"sp": sp, "tp": tpi},
            device_id_type=pl.DeviceIdType.MESH,
        )

    barrier = pltpu.get_barrier_semaphore()
    for k in range(n):
        for q in range(tp):
            if k or q:
                pl.semaphore_signal(
                    barrier,
                    inc=1,
                    device_id={"sp": (s + k) % n, "tp": (t + q) % tp},
                    device_id_type=pl.DeviceIdType.MESH,
                )
    fetches = [
        pltpu.make_async_copy(src, dst, local_sem.at[i])
        for i, (src, dst) in enumerate(
            ((blend_hbm, blend), (wg_hbm, wg), (wu_hbm, wu), (wd_hbm, wd))
        )
    ]
    for fetch in fetches:
        fetch.start()

    dt = jnp.log1p(jnp.exp(raw_ref[...]))
    la = extra_ref[...] - fade_ref[...] * dt
    row_i = lax.broadcasted_iota(jnp.int32, (length, length), 0)
    col_i = lax.broadcasted_iota(jnp.int32, (length, length), 1)
    lower = row_i >= col_i
    cum = jnp.dot(
        jnp.where(lower, 1.0, 0.0), la, precision=HIGHEST, preferred_element_type=F32
    )
    cum_t = first_dims(la, jnp.where(row_i <= col_i, 1.0, 0.0), HIGHEST)

    pl.semaphore_wait(barrier, n * tp - 1)

    sends = []
    following = (s + 1) % n
    tails = []
    for i, (src, dst) in enumerate(((x_ref, tail_x), (b_ref, tail_b), (c_ref, tail_c))):
        copy = remote(
            src.at[pl.ds(length - TAIL, TAIL)], dst, tail_ss.at[i], tail_rs.at[i], following, t
        )
        copy.start()
        tails.append(copy)
    meta_copies = []
    for k in range(n):
        for q in range(tp):
            if k or q:
                copy = remote(
                    meta_ref,
                    metas.at[k, q],
                    meta_ss.at[k, q],
                    meta_rs.at[k, q],
                    (s + k) % n,
                    (t + q) % tp,
                )
                copy.start()
                meta_copies.append(copy)
    metas[0, 0] = meta_ref[...]

    ext[TAIL:, 0:width] = x_ref[...].astype(F32)
    ext[TAIL:, width : width + STATE] = b_ref[...].astype(F32)
    ext[TAIL:, width + STATE : width + 2 * STATE] = c_ref[...].astype(F32)
    for copy in tails:
        copy.wait()
    inner = s > 0
    ext[0:TAIL, 0:width] = jnp.where(inner, tail_x[...].astype(F32), 0.0)
    ext[0:TAIL, width : width + STATE] = jnp.where(inner, tail_b[...].astype(F32), 0.0)
    ext[0:TAIL, width + STATE : width + 2 * STATE] = jnp.where(
        inner, tail_c[...].astype(F32), 0.0
    )

    def conv(taps, first, count):
        kernel_len = taps.shape[0]
        total = None
        for j in range(kernel_len):
            at = TAIL - kernel_len + 1 + j
            term = taps[j : j + 1, :] * ext[at : at + length, first : first + count]
            total = term if total is None else total + term
        return silu(total)

    keys = conv(kb_ref, width, STATE).astype(BF16)
    xdt = conv(kx_ref, 0, width) * spread(dt, width)
    tot = cum[length - 1 : length, :]
    remain = jnp.exp(tot - cum)
    state = first_dims(keys, (xdt * spread(remain, width)).astype(BF16))
    st_send[...] = state.astype(BF16)
    tot_send[...] = jnp.broadcast_to(spread(tot, width), tot_send.shape)
    states = []
    for k in range(1, n):
        a = remote(st_send, st_buf.at[k], st_ss.at[k], st_rs.at[k], (s + k) % n, t)
        b = remote(tot_send, tot_buf.at[k], tot_ss.at[k], tot_rs.at[k], (s + k) % n, t)
        b.start()
        a.start()
        states += [a, b]

    queries = conv(kc_ref, width + STATE, STATE).astype(BF16)
    scores = lax.dot_general(
        queries, keys, (((1,), (1,)), ((), ())), preferred_element_type=F32
    )
    xdt_b = xdt.astype(BF16)
    lane_head = lax.broadcasted_iota(jnp.int32, (length, width), 1) // HEAD_DIM
    mixed = jnp.zeros((length, width), F32)
    for h in range(heads):
        between = jnp.where(lower, cum[:, h : h + 1] - cum_t[h : h + 1, :], -1e30)
        weights = (scores * jnp.exp(between)).astype(BF16)
        chosen = jnp.where(lane_head == h, xdt_b, jnp.zeros_like(xdt_b))
        mixed = mixed + jnp.dot(weights, chosen, preferred_element_type=F32)
    reach = jnp.exp(spread(cum, width))
    modulation = silu(z_ref[...].astype(F32))

    for copy in states:
        copy.wait()
    incoming = jnp.zeros((STATE, width), F32)
    for k in range(n - 1, 0, -1):
        later = incoming * jnp.exp(tot_buf[k, 0:1, :]) + st_buf[k].astype(F32)
        incoming = jnp.where(k <= s, later, incoming)
    outside = jnp.dot(queries, incoming.astype(BF16), preferred_element_type=F32)
    g_send[...] = ((mixed + outside * reach) * modulation).astype(BF16)
    spreads = []
    for q in (2, 3, 1) if tp == 4 else range(1, tp):
        to = (t + q) % tp
        copy = remote(
            g_send.at[pl.ds(to * rows, rows)], g_buf.at[t], g_ss.at[q], g_rs.at[q], s, to
        )
        copy.start()
        spreads.append(copy)
    g_buf[t] = g_send[pl.ds(pl.multiple_of(t * rows, rows), rows), :]

    own_meta = meta_ref[...]
    onehots = []
    for k in range(n):
        first = ((s + k) % n * locals_).astype(F32)
        onehots.append(routing(own_meta, first, rows, cap, locals_).astype(BF16))
    for copy in meta_copies:
        copy.wait()
    fetches[0].wait()
    for copy in spreads:
        copy.wait()
    squares = jnp.zeros((rows, 1), F32)
    for i in range(tp):
        piece = g_buf[i].astype(F32)
        squares = squares + jnp.sum(piece * piece, axis=1, keepdims=True)
    scale = lax.rsqrt(squares / (tp * width) + EPS)
    projected = carry_ref[...].astype(F32)
    for i in range(tp):
        span = slice(i * width, (i + 1) * width)
        normed = (g_buf[i].astype(F32) * scale * gain_ref[:, span]).astype(BF16)
        projected = projected + jnp.dot(normed, blend[span, :], preferred_element_type=F32)
    middle = projected.astype(BF16)
    mid[...] = middle
    wide = middle.astype(F32)
    expert_in = (
        wide
        * lax.rsqrt(jnp.mean(wide * wide, axis=1, keepdims=True) + EPS)
        * sgain_ref[...]
    ).astype(BF16)

    order = []
    for k in range(n // 2 + 1):
        for other in (k, (n - k) % n):
            if other not in order:
                order.append(other)

    z_copies, far_copies, near_copies, p1_copies, p2_copies, ret_copies = {}, {}, {}, {}, {}, {}
    for k in order[1:] + order[:1]:
        picked = jnp.dot(onehots[k], expert_in, preferred_element_type=F32).astype(BF16)
        if k == 0:
            arr[0, t] = picked
        else:
            x_send[k] = picked
            z_copies[k] = remote(
                x_send.at[k], arr.at[k, t], z_ss.at[k], z_rs.at[k], (s + k) % n, t
            )
            z_copies[k].start()

    def pass_far(k):
        if k:
            z_copies[k].wait()
        far_copies[k] = remote(arr.at[k, t], arr.at[k, t], far_ss.at[k], far_rs.at[k], s, far)
        far_copies[k].start()
        first = remote(
            arr.at[k, t], arr.at[k, t], near_ss.at[k, 0], near_rs.at[k, 0], s, near
        )
        first.start()
        near_copies[k] = [first]

    def pass_near(k):
        far_copies[k].wait()
        second = remote(
            arr.at[k, far], arr.at[k, far], near_ss.at[k, 1], near_rs.at[k, 1], s, near
        )
        second.start()
        near_copies[k].append(second)

    weight_row0 = s * locals_

    def slot_weights(k):
        columns = [[] for _ in range(locals_)]
        for i in range(tp):
            q = (t + tp - i) % tp
            meta = metas[k, q]
            onehot = routing(meta, weight_row0.astype(F32), rows, cap, locals_)
            for l in range(locals_):
                expert = (weight_row0 + l).astype(F32)
                lift0, lift1 = jnp.exp(meta[2:3, :rows]), jnp.exp(meta[3:4, :rows])
                share = meta[4:5, :rows] / (lift0 + lift1)
                mine = share * (
                    jnp.where(meta[0:1, :rows] == expert, lift0, 0.0)
                    + jnp.where(meta[1:2, :rows] == expert, lift1, 0.0)
                )
                columns[l].append(jnp.sum(onehot * mine, axis=1, keepdims=True))
        return [jnp.concatenate(c, axis=0) for c in columns]

    def experts(k):
        shares = slot_weights(k)
        for copy in near_copies[k]:
            copy.wait()
        tokens = arr[k].reshape(tp * cap, model)
        if not loaded:
            for fetch in fetches[1:]:
                fetch.wait()
            loaded.append(True)
        total = None
        for l in range(locals_):
            gate = jnp.dot(tokens, wg[l], preferred_element_type=F32)
            up = jnp.dot(tokens, wu[l], preferred_element_type=F32)
            hidden = (silu(gate) * up * shares[l]).astype(BF16)
            term = jnp.dot(hidden, wd[l], preferred_element_type=F32)
            total = term if total is None else total + term
        part[k] = total.astype(BF16).reshape(tp, cap, model)
        pair = []
        for i, owner in ((1, near_far), (0, near)):
            copy = remote(
                part.at[k, owner], rs1.at[k, i], p1_ss.at[k, i], p1_rs.at[k, i], s, near
            )
            copy.start()
            pair.append(copy)
        p1_copies[k] = pair

    def reduce_near(k):
        for copy in p1_copies[k]:
            copy.wait()
        far_send[k] = (part[k, far].astype(F32) + rs1[k, 1].astype(F32)).astype(BF16)
        p2_copies[k] = remote(far_send.at[k], rs2.at[k], p2_ss.at[k], p2_rs.at[k], s, far)
        p2_copies[k].start()

    def reduce_far(k):
        p2_copies[k].wait()
        total = (
            part[k, t].astype(F32) + rs1[k, 0].astype(F32) + rs2[k].astype(F32)
        ).astype(BF16)
        if k == 0:
            ret[0] = total
        else:
            ret_send[k] = total
            ret_copies[k] = remote(
                ret_send.at[k], ret.at[k], ret_ss.at[k], ret_rs.at[k], (s + n - k) % n, t
            )
            ret_copies[k].start()

    loaded = []
    pass_far(order[0])
    for i in range(n + 2):
        if i + 1 < n:
            pass_far(order[i + 1])
        if i < n:
            pass_near(order[i])
            experts(order[i])
        if 0 <= i - 1 < n:
            reduce_near(order[i - 1])
        if 0 <= i - 2 < n:
            reduce_far(order[i - 2])

    result = mid[...].astype(F32)
    for k in order:
        if k:
            ret_copies[k].wait()
        result = result + first_dims(onehots[k], ret[k])
    out_ref[...] = result.astype(BF16)


def per_device(
    n,
    tp,
    carryover_vector,
    channel_source_entries,
    final_modulation_vector,
    entering_basis_matrix,
    readout_basis_matrix,
    raw_stride_amount,
    extra_log_attenuation,
    channel_fading_rate,
    channel_source_kernel,
    entering_basis_kernel,
    readout_basis_kernel,
    modulated_rescaling_vector,
    blender_final_matrix,
    specialist_rescaling_vector,
    specialist_gating_matrices,
    widening_matrices,
    contracting_matrices,
    assigned_specialist_ids,
    specialist_choice_affinity,
    cluster_chance,
):
    length, width = channel_source_entries.shape
    rows, model = carryover_vector.shape
    locals_, _, hidden = specialist_gating_matrices.shape
    experts = n * locals_
    picks = assigned_specialist_ids.shape[1]
    assert tp == 4 and picks == 2 and entering_basis_matrix.shape[1] == STATE
    per_expert = 2 * rows * picks // experts
    group_size = experts // EXPERT_GROUPS
    if group_size <= locals_:
        cap = locals_ * per_expert // picks
    else:
        cap = locals_ * per_expert
    cap = -(-min(cap, rows) // 16) * 16
    own_ids = lax.dynamic_slice_in_dim(
        assigned_specialist_ids, lax.axis_index("tp") * rows, rows, 0
    )
    meta = jnp.concatenate(
        [
            own_ids.astype(F32),
            specialist_choice_affinity,
            cluster_chance[:, None],
            jnp.zeros((rows, 3), F32),
        ],
        axis=1,
    ).T
    meta = jnp.pad(meta, ((0, 0), (0, 128 - rows)))
    vmem = pl.BlockSpec(memory_space=pltpu.VMEM)
    hbm = pl.BlockSpec(memory_space=pl.ANY)
    dma = pltpu.SemaphoreType.DMA
    scratch = [
        pltpu.VMEM(blender_final_matrix.shape, BF16),
        pltpu.VMEM(specialist_gating_matrices.shape, BF16),
        pltpu.VMEM(widening_matrices.shape, BF16),
        pltpu.VMEM(contracting_matrices.shape, BF16),
        pltpu.VMEM((TAIL, width), BF16),
        pltpu.VMEM((TAIL, STATE), BF16),
        pltpu.VMEM((TAIL, STATE), BF16),
        pltpu.VMEM((TAIL + length, width + 2 * STATE), F32),
        pltpu.VMEM((STATE, width), BF16),
        pltpu.VMEM((8, width), F32),
        pltpu.VMEM((n, STATE, width), BF16),
        pltpu.VMEM((n, 8, width), F32),
        pltpu.VMEM((length, width), BF16),
        pltpu.VMEM((tp, rows, width), BF16),
        pltpu.VMEM((rows, model), BF16),
        pltpu.VMEM((n, tp, 8, 128), F32),
        pltpu.VMEM((n, cap, model), BF16),
        pltpu.VMEM((n, tp, cap, model), BF16),
        pltpu.VMEM((n, tp, cap, model), BF16),
        pltpu.VMEM((n, 2, cap, model), BF16),
        pltpu.VMEM((n, cap, model), BF16),
        pltpu.VMEM((n, cap, model), BF16),
        pltpu.VMEM((n, cap, model), BF16),
        pltpu.VMEM((n, cap, model), BF16),
        dma((4,)),
    ]
    for shape in ((3,), (n,), (n,), (n, tp), (tp,), (n,), (n,), (n, 2), (n, 2), (n,), (n,)):
        scratch += [dma(shape), dma(shape)]
    return pl.pallas_call(
        functools.partial(kernel, n, tp, cap),
        out_shape=jax.ShapeDtypeStruct((rows, model), BF16),
        in_specs=[vmem] * 11 + [hbm, vmem, hbm, hbm, hbm, vmem, vmem],
        out_specs=vmem,
        scratch_shapes=scratch,
        compiler_params=pltpu.CompilerParams(
            collective_id=0, has_side_effects=True, vmem_limit_bytes=60 * 1024 * 1024
        ),
    )(
        channel_source_entries,
        entering_basis_matrix,
        readout_basis_matrix,
        final_modulation_vector,
        raw_stride_amount,
        extra_log_attenuation,
        channel_fading_rate[None, :],
        channel_source_kernel,
        entering_basis_kernel,
        readout_basis_kernel,
        modulated_rescaling_vector[None, :],
        blender_final_matrix,
        specialist_rescaling_vector[None, :],
        specialist_gating_matrices,
        widening_matrices,
        contracting_matrices,
        meta,
        carryover_vector,
    )


def solution(mesh):
    return jax.shard_map(
        functools.partial(per_device, mesh.shape["sp"], mesh.shape["tp"]),
        mesh=mesh,
        in_specs=(
            P(("grp", "sp", "tp"), None),
            P(("grp", "sp"), "tp"),
            P(("grp", "sp"), "tp"),
            P(("grp", "sp"), "tp"),
            P(("grp", "sp"), "tp"),
            P(("grp", "sp"), "tp"),
            P(("grp", "sp"), "tp"),
            P("tp"),
            P(None, "tp"),
            P(None, "tp"),
            P(None, "tp"),
            P(),
            P(),
            P(),
            P("sp", None, "tp"),
            P("sp", None, "tp"),
            P("sp", "tp", None),
            P(("grp", "sp"), None),
            P(("grp", "sp", "tp"), None),
            P(("grp", "sp", "tp")),
        ),
        out_specs=P(("grp", "sp", "tp"), None),
        check_vma=False,
    )
```

time: 321 us -> 72.1 us (0.22)
  waiting for transfers between devices: 165 us -> 0 us
  Pallas kernels: 0 us -> 65 us
  blocking collectives: 57.9 us -> 0 us
  matrix products: 20.8 us -> 0 us
  local copies, waits for them, and re-layouts: 26.1 us -> 5.3 us
  other arithmetic: 19.1 us -> 1.52 us
  starting transfers between devices: 16.9 us -> 0 us
  between operations: 14.2 us -> 0.01 us
    unnamed x4 -> x0, waiting for transfers between devices: 84.5 us -> none
    pallas_call x0 -> x1, Pallas kernels: none -> 65 us  [per_device(): pl.pallas_call(functools.partial(kernel, n, tp, cap), out_shape=jax.Shape...]
    all_gather x1 -> x0, waiting for transfers between devices: 32.5 us -> none  [per_device(): arrived = lax.all_gather(received, 'tp', axis=2, tiled=True)]
    all_to_all x1 -> x0, blocking collectives: 30 us -> none  [per_device(): lax.all_to_all(outgoing, 'sp', split_axis=0, concat_axis=0, tiled=True)]
    all_to_all x1 -> x0, waiting for transfers between devices: 24.9 us -> none  [per_device(): lax.all_to_all(width_total, 'sp', split_axis=0, concat_axis=0, tiled=True)]
    reduce_scatter x1 -> x0, waiting for transfers between devices: 22.6 us -> none  [per_device(): lax.psum_scatter(jnp.dot(normed, weight_rows, preferred_element_type=jnp....]
    dot_general x7 -> x0, matrix products: 20.8 us -> none  [the longest x1 7.3 us: per_device(): jnp.einsum('slqcf,lfd->slqcd', hidden, contracting_matrices, preferred_el...]
    all_gather x1 -> x0, blocking collectives: 13.9 us -> none  [prefix(): lax.all_gather(part.astype(kind), axis)]
  transfers between devices with their start and end apart: 7 -> 0, of which waited for: 4 -> 0; matrix products, arithmetic and copies ran while one was open for 6% -> 0% of each run, Pallas kernels for 0% -> 0%
where the time goes in v1:
time: 72.1 us; the launch traced here: 71.8 us
  Pallas kernels  65 us (90%)
  local copies, waits for them, and re-layouts  5.3 us (7%)
  other arithmetic  1.52 us (2%)
    pallas_call x1, Pallas kernels, per_device(): pl.pallas_call(functools.partial(kernel, n, tp, cap), out_shape=jax.Shape...  65 us
    unnamed x3, local copies, waits for them, and re-layouts  4.63 us

profile of v1, /device:TPU:0, one launch (start us, length us, event | category | flops | bytes accessed | tf_op | source)
XLA Modules:
  0.0 71.8 jit_solution(17092756643468841821)
XLA Ops:
  0.0 0.8 %dynamic-slice_convert_fusion = f32[64,2]{0,1:T(2,128)S(1)} fusion(s32[256,2]{0,1:T(2,128)} %param.37, s32[]{:T(128)S(6)} %select_n.3), kind=kLoop, calls=%fused_computation.1 | loop fusion | flops 128 | bytes 1028 | tf_op jit(solution)/shard_map/convert_element_type | solution.py:467
  0.8 0.1 pad.8.clone
  0.8 0.8 %maximum_bitcast_fusion = f32[8,64]{1,0:T(8,128)S(1)} fusion(f32[64,1]{0,1:T(1,128)} %bitcast.9, f32[64,2]{0,1:T(2,128)} %param.38, f32[64,2]{0,1:T(2,128)S(1)} %dynamic-slice_convert_fusion, f32[8]{0:T(128)S(1)} %pad.8.clone), kind=kLoop, calls=%fused_computation | loop fusion | flops 1536 | bytes 3360 | tf_op jit(solution)/shard_map/transpose | solution.py:473
  1.6 0.6 pad.4.meta_ref
  2.2 1.5 %copy.21.raw_ref = f32[256,4]{1,0:T(8,128)} copy(f32[256,4]{0,1:T(4,128)} %param.25) | data formatting | bytes 8192 | tf_op args[5]
  3.7 1.5 %copy.22.extra_ref = f32[256,4]{1,0:T(8,128)} copy(f32[256,4]{0,1:T(4,128)} %param.26) | data formatting | bytes 8192 | tf_op args[6]
  5.2 65.0 %shard_map.190 = bf16[64,2048]{1,0:T(8,128)(2,1)} custom-call(bf16[256,256]{1,0:T(8,128)(2,1)} %x_ref.1, bf16[256,128]{1,0:T(8,128)(2,1)} %b_ref.1, bf16[256,128]{1,0:T(8,128)(2,1)} %c_ref.1, bf16[256,256]{1,0:T(8,128)(2,1)} %z_ref.1, f32[256,4]{1,0:T(8,128)} %copy.21.raw_ref, f32[256,4]{1,0:T(8,128)} %copy.22.extra_ref, f32[1,4]{1,0:T(1,128)} %bitcast.8, ...), custom_call_target="tpu_custom_call" | custom-call | tf_op jit(solution)/shard_map/pallas_call | solution.py:507
  70.1 1.7 %copy.24 = bf16[64,2048]{1,0:T(8,128)(2,1)} copy(bf16[64,2048]{1,0:T(8,128)(2,1)} %shard_map.190) | data formatting | bytes 524288
  (1 shorter events, 0.0 us)

commit v2 on v1

--- a/solution.py
+++ b/solution.py
@@ -24,6 +24,12 @@
 def first_dims(a, b, precision=None):
     return lax.dot_general(
         a, b, (((0,), (0,)), ((), ())), precision=precision, preferred_element_type=F32
+    )
+
+
+def last_dims(a, b):
+    return lax.dot_general(
+        a, b, (((1,), (1,)), ((), ())), precision=HIGHEST, preferred_element_type=F32
     )
 
 
@@ -73,7 +79,9 @@
     wg_hbm,
     wu_hbm,
     wd_hbm,
-    meta_ref,
+    ids_ref,
+    aff_ref,
+    chance_ref,
     carry_ref,
     out_ref,
     blend,
@@ -91,6 +99,7 @@
     g_send,
     g_buf,
     mid,
+    meta_ref,
     metas,
     x_send,
     arr,
@@ -163,15 +172,26 @@
     for fetch in fetches:
         fetch.start()
 
-    dt = jnp.log1p(jnp.exp(raw_ref[...]))
-    la = extra_ref[...] - fade_ref[...] * dt
+    dt_t = jnp.log1p(jnp.exp(raw_ref[...]))
+    la_t = extra_ref[...] - fade_ref[...] * dt_t
     row_i = lax.broadcasted_iota(jnp.int32, (length, length), 0)
     col_i = lax.broadcasted_iota(jnp.int32, (length, length), 1)
     lower = row_i >= col_i
-    cum = jnp.dot(
-        jnp.where(lower, 1.0, 0.0), la, precision=HIGHEST, preferred_element_type=F32
-    )
-    cum_t = first_dims(la, jnp.where(row_i <= col_i, 1.0, 0.0), HIGHEST)
+    cum = last_dims(jnp.where(lower, 1.0, 0.0), la_t)
+    dt = last_dims(jnp.where(row_i == col_i, 1.0, 0.0), dt_t)
+    cum_t = jnp.dot(
+        la_t,
+        jnp.where(row_i <= col_i, 1.0, 0.0),
+        precision=HIGHEST,
+        preferred_element_type=F32,
+    )
+    meta_ref[...] = jnp.zeros_like(meta_ref)
+    ids = ids_ref[:, 0:rows]
+    for i in range(1, tp):
+        ids = jnp.where(t == i, ids_ref[:, i * rows : (i + 1) * rows], ids)
+    meta_ref[0:2, 0:rows] = ids.astype(F32)
+    meta_ref[2:4, 0:rows] = aff_ref[...]
+    meta_ref[4:5, 0:rows] = chance_ref[...]
 
     pl.semaphore_wait(barrier, n * tp - 1)
 
@@ -459,19 +479,6 @@
     else:
         cap = locals_ * per_expert
     cap = -(-min(cap, rows) // 16) * 16
-    own_ids = lax.dynamic_slice_in_dim(
-        assigned_specialist_ids, lax.axis_index("tp") * rows, rows, 0
-    )
-    meta = jnp.concatenate(
-        [
-            own_ids.astype(F32),
-            specialist_choice_affinity,
-            cluster_chance[:, None],
-            jnp.zeros((rows, 3), F32),
-        ],
-        axis=1,
-    ).T
-    meta = jnp.pad(meta, ((0, 0), (0, 128 - rows)))
     vmem = pl.BlockSpec(memory_space=pltpu.VMEM)
     hbm = pl.BlockSpec(memory_space=pl.ANY)
     dma = pltpu.SemaphoreType.DMA
@@ -491,6 +498,7 @@
         pltpu.VMEM((length, width), BF16),
         pltpu.VMEM((tp, rows, width), BF16),
         pltpu.VMEM((rows, model), BF16),
+        pltpu.VMEM((8, 128), F32),
         pltpu.VMEM((n, tp, 8, 128), F32),
         pltpu.VMEM((n, cap, model), BF16),
         pltpu.VMEM((n, tp, cap, model), BF16),
@@ -507,7 +515,7 @@
     return pl.pallas_call(
         functools.partial(kernel, n, tp, cap),
         out_shape=jax.ShapeDtypeStruct((rows, model), BF16),
-        in_specs=[vmem] * 11 + [hbm, vmem, hbm, hbm, hbm, vmem, vmem],
+        in_specs=[vmem] * 11 + [hbm, vmem, hbm, hbm, hbm] + [vmem] * 4,
         out_specs=vmem,
         scratch_shapes=scratch,
         compiler_params=pltpu.CompilerParams(
@@ -518,9 +526,9 @@
         entering_basis_matrix,
         readout_basis_matrix,
         final_modulation_vector,
-        raw_stride_amount,
-        extra_log_attenuation,
-        channel_fading_rate[None, :],
+        raw_stride_amount.T,
+        extra_log_attenuation.T,
+        channel_fading_rate[:, None],
         channel_source_kernel,
         entering_basis_kernel,
         readout_basis_kernel,
@@ -530,7 +538,9 @@
         specialist_gating_matrices,
         widening_matrices,
         contracting_matrices,
-        meta,
+        assigned_specialist_ids.T,
+        specialist_choice_affinity.T,
+        cluster_chance[None, :],
         carryover_vector,
     )
 

time: 72.1 us -> 68 us (0.943)
  local copies, waits for them, and re-layouts: 5.3 us -> 2.98 us
  other arithmetic: 1.52 us -> 0 us
    unnamed x3 -> x1, local copies, waits for them, and re-layouts: 4.63 us -> 1.67 us
    broadcast_in_dim x1, local copies, waits for them, and re-layouts: 0.01 us -> 1.31 us  [per_device(): channel_fading_rate[:, None]]
    transpose x1 -> x0, other arithmetic: 0.76 us -> none  [per_device(): meta = jnp.concatenate([own_ids.astype(F32), specialist_choice_affinity,...]
    convert_element_type x1 -> x0, other arithmetic: 0.75 us -> none  [per_device(): own_ids.astype(F32)]
where the time goes in v2:
time: 68 us; the launch traced here: 67.9 us
  Pallas kernels  64.9 us (95%)
  local copies, waits for them, and re-layouts  2.98 us (4%)
    pallas_call x1, Pallas kernels, per_device(): pl.pallas_call(functools.partial(kernel, n, tp, cap), out_shape=jax.Shape...  64.9 us
    unnamed x1, local copies, waits for them, and re-layouts  1.67 us

profile of v2, /device:TPU:0, one launch (start us, length us, event | category | flops | bytes accessed | tf_op | source)
XLA Modules:
  0.0 67.9 jit_solution(18017526770802614621)
XLA Ops:
  0.0 1.3 %copy.21.fade_ref = f32[4,1]{1,0:T(4,128)} copy(f32[4,1]{0,1:T(1,128)} %bitcast.15) | data formatting | bytes 32 | tf_op jit(solution)/shard_map/broadcast_in_dim | solution.py:531
  1.3 64.9 %shard_map.190 = bf16[64,2048]{1,0:T(8,128)(2,1)} custom-call(bf16[256,256]{1,0:T(8,128)(2,1)} %x_ref.1, bf16[256,128]{1,0:T(8,128)(2,1)} %b_ref.1, bf16[256,128]{1,0:T(8,128)(2,1)} %c_ref.1, bf16[256,256]{1,0:T(8,128)(2,1)} %z_ref.1, f32[4,256]{1,0:T(4,128)} %bitcast.9, f32[4,256]{1,0:T(4,128)} %bitcast.10, f32[4,1]{1,0:T(4,128)} %copy.21.fade_ref, ...), custom_call_target="tpu_custom_call" | custom-call | tf_op jit(solution)/shard_map/pallas_call | solution.py:515
  66.2 1.7 %copy.23 = bf16[64,2048]{1,0:T(8,128)(2,1)} copy(bf16[64,2048]{1,0:T(8,128)(2,1)} %shard_map.190) | data formatting | bytes 524288
